TPU v7x, 512 devices: a whole 4x4x16 slice. The times are simulated.
512 devices in a mesh: ep: 32 (over z, core), tp: 16 (over y, x).
Axes of the slice: x: 4, y: 4, z: 16, core: 2. Of those that a mesh axis runs over, the one named last changes fastest.
Arguments:
- tokens: bfloat16 [512, 2048], P('ep'), may hold values from -6 to 6
- attn_gain: float32 [2048], replicated, may hold values from 0.1 to 1.9
- query_weight: bfloat16 [2048, 2048], P('ep', 'tp'), may hold values from -0.125 to 0.125
- key_weight: bfloat16 [2048, 2048], P('ep', 'tp'), may hold values from -0.125 to 0.125
- value_weight: bfloat16 [2048, 2048], P('ep', 'tp'), may hold values from -0.125 to 0.125
- forget_weight: bfloat16 [2048, 16], P(None, 'tp'), may hold values from -0.125 to 0.125
- forget_bias: float32 [16], P('tp'), may hold values from -1 to 2
- cache_keys: bfloat16 [512, 16, 384, 128], P('ep', 'tp'), may hold values from -240 to 240
- cache_values: bfloat16 [512, 16, 384, 128], P('ep', 'tp'), may hold values from -6 to 6
- cache_gates: float32 [512, 16, 384], P('ep', 'tp'), may hold values from -768 to 0, as said below
- lengths: int32 [512], P('ep'), may hold values from 1 to 384
- output_weight: bfloat16 [2048, 2048], P('tp', 'ep'), may hold values from -0.125 to 0.125
- ffn_gain: float32 [2048], replicated, may hold values from 0.1 to 1.9
- dense_gate_proj: bfloat16 [2048, 2048], P('ep', 'tp'), may hold values from -0.125 to 0.125
- dense_up_proj: bfloat16 [2048, 2048], P('ep', 'tp'), may hold values from -0.125 to 0.125
- dense_down_proj: bfloat16 [2048, 2048], P('tp', 'ep'), may hold values from -0.125 to 0.125
- dense_mix: bfloat16 [2048], replicated, may hold values from -0.125 to 0.125
- expert_ids: int32 [512, 2], P('ep'), may hold values from 0 to 31, as said below
- group_prob: float32 [512], P('ep'), may hold values from 0.25 to 1
- pair_prob: float32 [512, 2], P('ep'), may hold values from 0.05 to 1
- expert_gate: bfloat16 [32, 2048, 2048], P('ep', None, 'tp'), may hold values from -0.125 to 0.125
- expert_up: bfloat16 [32, 2048, 2048], P('ep', None, 'tp'), may hold values from -0.125 to 0.125
- expert_down: bfloat16 [32, 2048, 2048], P('ep', 'tp'), may hold values from -0.125 to 0.125
Outputs:
- mixed_out: bfloat16 [512, 2048], P('ep')
Inputs may be any that keep to these rules, and one draw needn't show every extreme that they name: `expert_ids`: each row names two different experts of one group, the groups being 4 runs of consecutive ids. In each aligned block of 16 rows (the rows of one index of ep) no expert is named more than 2 times, and some expert exactly 2 times. `cache_gates`: along positions the values never rise.
All inputs are finite; a program needn't handle non-finite values.
Results may differ from a plain program's by a relative error of at most 0.014.
Values may be sent and summed in bfloat16 or wider, within the bound.
No kernel may reach another device: no remote copies, remote signals or barrier semaphores. Data moves between devices by JAX's collectives and lax.ppermute only.
A program may use at most 64 MiB of HBM per device.

v0:
```python
import math

import jax
import jax.numpy as jnp
from jax import lax
from jax.sharding import Mesh
from jax.sharding import PartitionSpec as P

EP = ("ep_0", "ep_1")


EPSILON = 1e-06


def sent_together(arrays, axis, dim, along):
    widths = [a.shape[along] for a in arrays]
    both = jnp.concatenate(arrays, axis=along)
    filled = lax.all_gather(both, axis, axis=dim, tiled=True)
    return tuple(jnp.split(filled, [sum(widths[:k]) for k in range(1, len(widths))], axis=along))


def from_everyone(array, axis):
    copies = jnp.broadcast_to(array, (lax.axis_size(axis), *array.shape))
    return lax.all_to_all(copies, axis, split_axis=0, concat_axis=0, tiled=True)


def laid_out(pieces, dim):
    lengths = list(pieces.shape[1:])
    lengths[dim] *= pieces.shape[0]
    return jnp.moveaxis(pieces, 0, dim).reshape(lengths)


def collect(array, axis, dim):
    pieces = from_everyone(array, axis)
    return laid_out(pieces, dim)


def taken_together(array, axis):
    everything = from_everyone(array, axis)
    return jnp.sum(everything.astype(jnp.float32), axis=0)


def gather_in_order(array, axes, sequence):
    pieces = array[None]
    for k in sequence:
        pieces = lax.all_gather(pieces, axes[k], axis=0, tiled=True)
    held = [lax.axis_size(axes[k]) for k in reversed(sequence)]
    pieces = pieces.reshape(*held, *array.shape)
    turned = sorted(range(len(sequence)), key=lambda place: sequence[len(sequence) - 1 - place])
    return pieces.transpose(*turned, *range(len(sequence), pieces.ndim)).reshape(-1, *array.shape)


def gathered_by_axis(array, axes, sequence, dim):
    return laid_out(gather_in_order(array, axes, sequence), dim)


def rms_scale(values, norm_gain):
    widened = values.astype(jnp.float32)
    return (
        widened
        * lax.rsqrt(jnp.mean(widened * widened, axis=-1, keepdims=True) + EPSILON)
        * norm_gain
    )


def attend(queries, keys_new, values_new, key_cache, value_cache, gate_cache, lengths, log_forget):
    cache_span = key_cache.shape[2]
    score_scale = 1.0 / math.sqrt(key_cache.shape[3])
    positions = jnp.arange(cache_span, dtype=jnp.int32)
    live_mask = positions[None, :] < lengths[:, None]
    last_mask = positions[None, :] == lengths[:, None] - 1
    last_gate = jnp.sum(jnp.where(last_mask[:, None, :], gate_cache, 0.0), axis=-1)
    gate_now = last_gate + log_forget
    scores = (
        jnp.einsum("shd,shpd->shp", queries, key_cache, preferred_element_type=jnp.float32)
        * score_scale
    )
    scores = scores + gate_now[:, :, None] - gate_cache
    scores = jnp.where(live_mask[:, None, :], scores, -jnp.inf)
    own_score = (
        jnp.sum(queries.astype(jnp.float32) * keys_new.astype(jnp.float32), axis=-1) * score_scale
    )
    row_top = jnp.maximum(jnp.max(scores, axis=-1), own_score)
    raised = jnp.exp(scores - row_top[:, :, None])
    own_raised = jnp.exp(own_score - row_top)
    totals = jnp.sum(raised, axis=-1) + own_raised
    weights_low = (raised / totals[:, :, None]).astype(jnp.bfloat16)
    own_prob = (own_raised / totals).astype(jnp.bfloat16)
    attended = jnp.einsum(
        "shp,shpd->shd", weights_low, value_cache, preferred_element_type=jnp.float32
    )
    attended = attended + own_prob.astype(jnp.float32)[:, :, None] * values_new.astype(jnp.float32)
    return attended.astype(jnp.bfloat16)


def column_fold(source, pieces):
    return tuple(
        (
            jnp.dot(source, weight_piece, preferred_element_type=jnp.float32)
            for weight_piece in pieces
        )
    )


def right_product(left_rows, weight_piece):
    return jnp.dot(left_rows, weight_piece, preferred_element_type=jnp.float32)


def shards(
    tokens,
    attn_gain,
    query_weight,
    key_weight,
    value_weight,
    forget_weight,
    forget_bias,
    cache_keys,
    cache_values,
    cache_gates,
    lengths,
    output_weight,
    ffn_gain,
    dense_gate_proj,
    dense_up_proj,
    dense_down_proj,
    dense_mix,
    expert_ids,
    group_prob,
    pair_prob,
    expert_gate,
    expert_up,
    expert_down,
):
    seq_count = tokens.shape[0]
    head_count = cache_keys.shape[1]
    head_size = cache_keys.shape[3]
    normed = rms_scale(tokens, attn_gain).astype(jnp.bfloat16)
    projected = column_fold(
        normed, sent_together((query_weight, key_weight, value_weight), EP, 0, 1)
    )
    queries = projected[0].astype(jnp.bfloat16).reshape(seq_count, head_count, head_size)
    keys_new = projected[1].astype(jnp.bfloat16).reshape(seq_count, head_count, head_size)
    values_new = projected[2].astype(jnp.bfloat16).reshape(seq_count, head_count, head_size)
    log_forget = jax.nn.log_sigmoid(
        jnp.dot(normed, forget_weight, preferred_element_type=jnp.float32) + forget_bias
    )
    attended = attend(
        queries, keys_new, values_new, cache_keys, cache_values, cache_gates, lengths, log_forget
    )
    attended = attended.reshape(seq_count, head_count * head_size)
    head_terms = right_product(attended, collect(output_weight, EP, 1))
    mixed_heads = taken_together(head_terms.astype(jnp.bfloat16), "tp").astype(jnp.float32)
    residual = (tokens.astype(jnp.float32) + mixed_heads).astype(jnp.bfloat16)
    ffn_in = rms_scale(residual, ffn_gain).astype(jnp.bfloat16)
    dense_parts = column_fold(ffn_in, sent_together((dense_gate_proj, dense_up_proj), EP, 0, 1))
    dense_hidden = (jax.nn.silu(dense_parts[0]) * dense_parts[1]).astype(jnp.bfloat16)
    dense_terms = right_product(dense_hidden, gathered_by_axis(dense_down_proj, EP, (0, 1), 1))
    mix = jax.nn.sigmoid(jnp.dot(ffn_in, dense_mix, preferred_element_type=jnp.float32))
    expert_count = lax.axis_size(EP) * expert_gate.shape[0]
    capacity = 4 * seq_count // expert_count
    slot_total = expert_count * capacity
    picks = expert_ids.reshape(-1)
    expert_grid = jnp.arange(expert_count, dtype=jnp.int32)
    pick_onehot = (picks[:, None] == expert_grid[None, :]).astype(jnp.int32)
    earlier = jnp.cumsum(pick_onehot, axis=0) - pick_onehot
    slot_rank = jnp.sum(earlier * pick_onehot, axis=1)
    destination = (picks * capacity + slot_rank).reshape(seq_count, 2)
    slot_grid = jnp.arange(slot_total, dtype=jnp.int32)
    select_first = (destination[:, 0:1] == slot_grid[None, :]).astype(jnp.bfloat16)
    select_second = (destination[:, 1:2] == slot_grid[None, :]).astype(jnp.bfloat16)
    selector = select_first + select_second
    outbound = jnp.einsum("sk,sd->kd", selector, ffn_in, preferred_element_type=jnp.float32)
    outbound = outbound.astype(jnp.bfloat16).reshape(expert_count, capacity, ffn_in.shape[1])
    arrived = lax.all_to_all(outbound, EP, split_axis=0, concat_axis=0, tiled=True)
    sources, slots_now, feature = arrived.shape
    row_data = arrived.reshape(sources * slots_now, feature)
    gate_part = jnp.dot(row_data, expert_gate[0], preferred_element_type=jnp.float32)
    up_part = jnp.dot(row_data, expert_up[0], preferred_element_type=jnp.float32)
    expert_hidden = (jax.nn.silu(gate_part) * up_part).astype(jnp.bfloat16)
    partial_out = jnp.dot(expert_hidden, expert_down[0], preferred_element_type=jnp.float32)
    returned = lax.all_to_all(
        partial_out.reshape(sources, slots_now, feature).astype(jnp.bfloat16),
        EP,
        split_axis=0,
        concat_axis=0,
        tiled=True,
    ).astype(jnp.float32)
    returned = returned.reshape(slot_total, ffn_in.shape[1])
    routes = group_prob[:, None] * pair_prob / jnp.sum(pair_prob, axis=1, keepdims=True)
    first_back = returned[destination[:, 0]]
    second_back = returned[destination[:, 1]]
    side_total = (
        routes[:, 0:1] * first_back + routes[:, 1:2] * second_back + mix[:, None] * dense_terms
    )
    side_total = taken_together(side_total.astype(jnp.bfloat16), "tp").astype(jnp.float32)
    result = residual.astype(jnp.float32) + side_total
    return result.astype(jnp.bfloat16)


def solution(mesh):
    finer = Mesh(mesh.devices.reshape(16, 2, mesh.shape["tp"]), ("ep_0", "ep_1", "tp"))
    in_specs = (
        P(EP, None),
        P(),
        P(EP, "tp"),
        P(EP, "tp"),
        P(EP, "tp"),
        P(None, "tp"),
        P("tp"),
        P(EP, "tp", None, None),
        P(EP, "tp", None, None),
        P(EP, "tp", None),
        P(EP),
        P("tp", EP),
        P(),
        P(EP, "tp"),
        P(EP, "tp"),
        P("tp", EP),
        P(),
        P(EP, None),
        P(EP),
        P(EP, None),
        P(EP, None, "tp"),
        P(EP, None, "tp"),
        P(EP, "tp", None),
    )
    out_specs = P(EP, None)
    return jax.shard_map(
        shards, mesh=finer, in_specs=in_specs, out_specs=out_specs, check_vma=False
    )
```

profile of v0, /device:TPU:1, one launch (start us, length us, event | category | flops | bytes accessed | tf_op | source)
XLA Modules:
  0.0 240.2 jit_solution(12965718424162420117)
XLA Ops:
  6.6 1.5 pad_maximum_fusion
  8.1 1.6 broadcast_in_dim.17
  9.7 16.7 %all-to-all-start = ((bf16[32,128,64]{1,2,0:T(8,128)(2,1)}), bf16[32,128,64]{1,2,0:T(8,128)(2,1)S(1)}, u32[]{:S(2)}, u32[]{:S(2)}) async-start(bf16[32,128,64]{1,2,0:T(8,128)(2,1)} %broadcast_in_dim.17), calls=%async_computation | async-start | bytes 1048576 | tf_op jit(solution)/shard_map/all_to_all | solution.py:24
  27.3 0.3 fusion.45
  27.8 63.6 %all-gather.4.cloned.1.call-done = bf16[2048,384]{1,0:T(8,128)(2,1)} async-done(((bf16[64,384]{1,0:T(8,128)(2,1)}), bf16[2048,384]{1,0:T(8,128)(2,1)}) %all-gather.4.cloned.1.call-update) | async-done | bytes 1572880 | tf_op jit(solution)/shard_map/all_gather | solution.py:18
  91.4 1.4 convolution_convert_fusion.5
  92.8 1.4 fusion.14
  94.2 0.6 fusion.4
  94.9 0.3 fusion.82
  95.2 0.3 fusion.70
  95.6 0.4 fusion.2
  96.0 1.5 convolution_convert_fusion.2
  97.5 1.1 broadcast_in_dim.18
  98.6 6.6 %all-to-all-start.1 = ((bf16[16,16,2048]{2,1,0:T(8,128)(2,1)}), bf16[16,16,2048]{2,1,0:T(8,128)(2,1)S(1)}, u32[]{:S(2)}, u32[]{:S(2)}) async-start(bf16[16,16,2048]{2,1,0:T(8,128)(2,1)} %broadcast_in_dim.18), calls=%async_computation.1 | async-start | bytes 2097152 | tf_op jit(solution)/shard_map/all_to_all | solution.py:24
  106.0 15.7 %all-to-all-done.1 = bf16[16,16,2048]{2,1,0:T(8,128)(2,1)S(1)} async-done(((bf16[16,16,2048]{2,1,0:T(8,128)(2,1)}), bf16[16,16,2048]{2,1,0:T(8,128)(2,1)S(1)}, u32[]{:S(2)}, u32[]{:S(2)}) %all-to-all-start.1) | async-done | bytes 1048608 | tf_op jit(solution)/shard_map/all_to_all | solution.py:24
  122.0 0.3 convolution_convert_fusion.1
  122.3 0.9 reshape.216
  123.2 10.1 %all-to-all-start.2 = ((bf16[32,2,2048]{2,1,0:T(2,128)(2,1)}), bf16[32,2,2048]{2,1,0:T(2,128)(2,1)S(1)}, u32[]{:S(2)}, u32[]{:S(2)}) async-start(bf16[32,2,2048]{2,1,0:T(2,128)(2,1)} %reshape.216), calls=%async_computation.2 | async-start | bytes 524288 | tf_op jit(solution)/shard_map/all_to_all | solution.py:174
  133.3 0.6 pad_maximum_fusion.1
  134.0 32.8 %all-gather = bf16[2048,64]{0,1:T(8,128)(2,1)S(1)} all-gather(bf16[128,64]{0,1:T(8,128)(2,1)S(1)} %copy-done.6), channel_id=2, replica_groups=mesh['ep_0'=16,'ep_1'=2,'tp'=16] {'ep_0'}, dimensions={0}, use_global_device_ids=true | all-gather | bytes 278528 | tf_op jit(solution)/shard_map/all_gather | solution.py:46
  166.9 7.8 %all_gather.15 = bf16[32,128,64]{1,0,2:T(8,128)(2,1)S(1)} all-gather(bf16[16,128,64]{1,0,2:T(8,128)(2,1)S(1)} %bitcast.83), channel_id=1, replica_groups=mesh['ep_0'=16,'ep_1'=2,'tp'=16] {'ep_1'}, dimensions={0}, use_global_device_ids=true | all-gather | bytes 786432 | tf_op jit(solution)/shard_map/all_gather | solution.py:46
  175.3 1.3 fusion.6
  176.8 1.0 copy.64
  177.8 10.6 %all-to-all-start.3 = ((bf16[32,2,2048]{2,1,0:T(2,128)(2,1)}), bf16[32,2,2048]{2,1,0:T(2,128)(2,1)S(1)}, u32[]{:S(2)}, u32[]{:S(2)}) async-start(bf16[32,2,2048]{2,1,0:T(2,128)(2,1)} %copy.64), calls=%async_computation.3 | async-start | bytes 524288 | tf_op jit(solution)/shard_map/all_to_all | solution.py:181
  188.7 17.2 %all-gather.6.cloned.1.call-done = bf16[2048,256]{1,0:T(8,128)(2,1)} async-done(((bf16[64,256]{1,0:T(8,128)(2,1)}), bf16[2048,256]{1,0:T(8,128)(2,1)}) %all-gather.6.cloned.1.call-update) | async-done | bytes 1048592 | tf_op jit(solution)/shard_map/all_gather | solution.py:18
  205.9 1.3 fusion.23
  207.2 3.8 %all-to-all-done.3 = bf16[32,2,2048]{2,1,0:T(2,128)(2,1)S(1)} async-done(((bf16[32,2,2048]{2,1,0:T(2,128)(2,1)}), bf16[32,2,2048]{2,1,0:T(2,128)(2,1)S(1)}, u32[]{:S(2)}, u32[]{:S(2)}) %all-to-all-start.3) | async-done | bytes 262176 | tf_op jit(solution)/shard_map/all_to_all | solution.py:181
  211.1 0.6 gather_fusion
  211.7 0.6 gather_fusion.1
  212.3 1.5 fusion.1
  213.9 18.7 %all_to_all.25 = bf16[16,16,2048]{2,1,0:T(8,128)(2,1)S(1)} all-to-all(bf16[16,16,2048]{2,1,0:T(8,128)(2,1)S(1)} %broadcast_in_dim.20), channel_id=1, replica_groups=mesh['ep_0'=16,'ep_1'=2,'tp'=16] {'tp'}, dimensions={0} | all-to-all | bytes 2097152 | tf_op jit(solution)/shard_map/all_to_all | solution.py:24
  232.8 0.6 fusion.40
  (73 shorter events, 3.0 us)
Async XLA Ops:
  6.5 87.7 %copy-start = (bf16[16,1,384,128]{3,2,1,0:T(8,128)(2,1)S(1)}, bf16[16,1,384,128]{3,2,1,0:T(8,128)(2,1)}, u32[]{:S(2)}) copy-start(bf16[16,1,384,128]{3,2,1,0:T(8,128)(2,1)} %param.30) | copy-start | bytes 4718596
  6.5 20.6 %copy-start.1 = (bf16[16,2048]{1,0:T(8,128)(2,1)S(1)}, bf16[16,2048]{1,0:T(8,128)(2,1)}, u32[]{:S(2)}) copy-start(bf16[16,2048]{1,0:T(8,128)(2,1)} %param.23) | copy-start | bytes 196612
  6.5 20.7 %copy-start.13 = (s32[16]{0:T(128)S(1)}, s32[16]{0:T(128)}, u32[]{:S(2)}) copy-start(s32[16]{0:T(128)} %param.33) | copy-start | bytes 196
  6.5 20.8 %copy-start.4 = (f32[16,1,384]{2,1,0:T(1,128)S(1)}, f32[16,1,384]{2,1,0:T(1,128)}, u32[]{:S(2)}) copy-start(f32[16,1,384]{2,1,0:T(1,128)} %param.32) | copy-start | bytes 73732
  6.5 21.0 %copy-start.9 = (f32[2048]{0:T(1024)S(1)}, f32[2048]{0:T(1024)}, u32[]{:S(2)}) copy-start(f32[2048]{0:T(1024)} %param.24) | copy-start | bytes 24580
  6.5 21.1 %copy-start.16 = (bf16[2048,1]{0,1:T(2,128)(2,1)S(1)}, bf16[2048,1]{0,1:T(2,128)(2,1)}, u32[]{:S(2)}) copy-start(bf16[2048,1]{0,1:T(2,128)(2,1)} %param.28) | copy-start | bytes 12292
  6.6 84.8 %all-gather.4.cloned.1.call-start = ((), (), s32[]{:S(2)}) async-start(), calls=%async_computation.5 | async-start | bytes 1622016 | tf_op jit(solution)/shard_map/all_gather | solution.py:18
  9.7 86.3 %all-to-all-start = ((bf16[32,128,64]{1,2,0:T(8,128)(2,1)}), bf16[32,128,64]{1,2,0:T(8,128)(2,1)S(1)}, u32[]{:S(2)}, u32[]{:S(2)}) async-start(bf16[32,128,64]{1,2,0:T(8,128)(2,1)} %broadcast_in_dim.17), calls=%async_computation | async-start | bytes 1048576 | tf_op jit(solution)/shard_map/all_to_all | solution.py:24
  91.4 4.2 %copy-start.15 = (bf16[16,1,384,128]{3,2,1,0:T(8,128)(2,1)S(1)}, bf16[16,1,384,128]{3,2,1,0:T(8,128)(2,1)}, u32[]{:S(2)}) copy-start(bf16[16,1,384,128]{3,2,1,0:T(8,128)(2,1)} %param.31) | copy-start | bytes 4718596
  97.5 7.7 %copy-start.11 = (s32[16,2]{0,1:T(2,128)S(1)}, s32[16,2]{0,1:T(2,128)}, u32[]{:S(2)}) copy-start(s32[16,2]{0,1:T(2,128)} %param.40) | copy-start | bytes 388
  98.6 23.3 %copy-start.5 = (f32[2048]{0:T(1024)S(1)}, f32[2048]{0:T(1024)}, u32[]{:S(2)}) copy-start(f32[2048]{0:T(1024)} %param.35) | copy-start | bytes 24580
  98.6 23.0 %all-to-all-start.1 = ((bf16[16,16,2048]{2,1,0:T(8,128)(2,1)}), bf16[16,16,2048]{2,1,0:T(8,128)(2,1)S(1)}, u32[]{:S(2)}, u32[]{:S(2)}) async-start(bf16[16,16,2048]{2,1,0:T(8,128)(2,1)} %broadcast_in_dim.18), calls=%async_computation.1 | async-start | bytes 2097152 | tf_op jit(solution)/shard_map/all_to_all | solution.py:24
  105.2 28.1 %copy-start.7 = (bf16[64,128]{1,0:T(8,128)(2,1)S(1)}, bf16[64,128]{1,0:T(8,128)(2,1)}, u32[]{:S(2)}) copy-start(bf16[64,128]{1,0:T(8,128)(2,1)} %param.37) | copy-start | bytes 49156
  105.2 28.1 %copy-start.8 = (bf16[64,128]{1,0:T(8,128)(2,1)S(1)}, bf16[64,128]{1,0:T(8,128)(2,1)}, u32[]{:S(2)}) copy-start(bf16[64,128]{1,0:T(8,128)(2,1)} %param.36) | copy-start | bytes 49156
  105.3 28.7 %copy-start.10 = (bf16[2048]{0:T(1024)(128)(2,1)S(1)}, bf16[2048]{0:T(1024)(128)(2,1)}, u32[]{:S(2)}) copy-start(bf16[2048]{0:T(1024)(128)(2,1)} %param.39) | copy-start | bytes 12292
  105.3 28.8 %copy-start.6 = (bf16[128,64]{0,1:T(8,128)(2,1)S(1)}, bf16[128,64]{0,1:T(8,128)(2,1)}, u32[]{:S(2)}) copy-start(bf16[128,64]{0,1:T(8,128)(2,1)} %param.38) | copy-start | bytes 49156
  123.2 51.7 %copy-start.12 = (f32[16,2]{0,1:T(2,128)S(1)}, f32[16,2]{0,1:T(2,128)}, u32[]{:S(2)}) copy-start(f32[16,2]{0,1:T(2,128)} %param.42) | copy-start | bytes 388
  123.2 51.8 %all-to-all-start.2 = ((bf16[32,2,2048]{2,1,0:T(2,128)(2,1)}), bf16[32,2,2048]{2,1,0:T(2,128)(2,1)S(1)}, u32[]{:S(2)}, u32[]{:S(2)}) async-start(bf16[32,2,2048]{2,1,0:T(2,128)(2,1)} %reshape.216), calls=%async_computation.2 | async-start | bytes 524288 | tf_op jit(solution)/shard_map/all_to_all | solution.py:174
  133.2 72.6 %all-gather.6.cloned.1.call-start = ((), (), s32[]{:S(2)}) async-start(), calls=%async_computation.6 | async-start | bytes 1081344 | tf_op jit(solution)/shard_map/all_gather | solution.py:18
  134.0 41.0 %copy-start.2 = (bf16[1,2048,128]{2,1,0:T(8,128)(2,1)S(1)}, bf16[1,2048,128]{2,1,0:T(8,128)(2,1)}, u32[]{:S(2)}) copy-start(bf16[1,2048,128]{2,1,0:T(8,128)(2,1)} %param.43) | copy-start | bytes 1572868
  175.1 1.5 copy-start.3
  175.1 13.4 %copy-start.14 = (f32[16]{0:T(128)S(1)}, f32[16]{0:T(128)}, u32[]{:S(2)}) copy-start(f32[16]{0:T(128)} %param.41) | copy-start | bytes 196
  177.8 33.2 %all-to-all-start.3 = ((bf16[32,2,2048]{2,1,0:T(2,128)(2,1)}), bf16[32,2,2048]{2,1,0:T(2,128)(2,1)S(1)}, u32[]{:S(2)}, u32[]{:S(2)}) async-start(bf16[32,2,2048]{2,1,0:T(2,128)(2,1)} %copy.64), calls=%async_computation.3 | async-start | bytes 524288 | tf_op jit(solution)/shard_map/all_to_all | solution.py:181
Sparse Core Ops, SparseCore 0:
  9.5 81.8 all-gather.3
  136.2 69.6 all-gather.5
where the time goes:
time: 241 us; the launch traced here: 240 us
  waiting for transfers between devices  100 us (41%)
  blocking collectives  59.3 us (25%)
  starting transfers between devices  44.1 us (18%)
  between operations  14.4 us (6%)
  matrix products  10.6 us (4%)
  local copies, waits for them, and re-layouts  6.76 us (3%)
  other arithmetic  4.7 us (2%)
    all_gather x2, waiting for transfers between devices, sent_together(): filled = lax.all_gather(both, axis, axis=dim, tiled=True)  80.8 us
    all_gather x2, blocking collectives, gather_in_order(): pieces = lax.all_gather(pieces, axes[k], axis=0, tiled=True)  40.6 us
    all_to_all x2, starting transfers between devices, from_everyone(): return lax.all_to_all(copies, axis, split_axis=0, concat_axis=0, tiled=True)  23.3 us
    all_to_all x1, blocking collectives, from_everyone(): return lax.all_to_all(copies, axis, split_axis=0, concat_axis=0, tiled=True)  18.7 us
    all_to_all x2, waiting for transfers between devices, from_everyone(): return lax.all_to_all(copies, axis, split_axis=0, concat_axis=0, tiled=True)  15.7 us
    all_to_all x1, starting transfers between devices, shards(): lax.all_to_all(partial_out.reshape(sources, slots_now, feature).astype(jn...  10.6 us
    all_to_all x1, starting transfers between devices, shards(): lax.all_to_all(outbound, EP, split_axis=0, concat_axis=0, tiled=True)  10.1 us
  transfers between devices with their start and end apart: 6, of which 4 were waited for; matrix products, arithmetic and copies ran while one was open for 5% of the time, Pallas kernels for 0%

commit v1 on v0

v1 whole, which is shorter than its diff:
```python
import math

import jax
import jax.numpy as jnp
from jax import lax
from jax.sharding import Mesh
from jax.sharding import PartitionSpec as P

EP = ("zh", "zl", "c")
Z = ("zh", "zl")
TP = ("y", "x")
EPSILON = 1e-06


def exchanged(pieces, axes):
    return lax.all_to_all(pieces, axes, split_axis=0, concat_axis=0, tiled=True)


def summed_over(array, axes):
    copies = jnp.broadcast_to(array, (lax.axis_size(axes), *array.shape))
    return jnp.sum(exchanged(copies, axes).astype(jnp.float32), axis=0)


def product(left, right):
    return jnp.dot(left, right, preferred_element_type=jnp.float32)


def product_transposed(left, right):
    return lax.dot_general(
        left, right, (((1,), (1,)), ((), ())), preferred_element_type=jnp.float32
    )


def rms_scale(values, norm_gain):
    widened = values.astype(jnp.float32)
    return (
        widened
        * lax.rsqrt(jnp.mean(widened * widened, axis=-1, keepdims=True) + EPSILON)
        * norm_gain
    )


def attend(queries, keys_new, values_new, key_cache, value_cache, gate_cache, lengths, log_forget):
    cache_span = key_cache.shape[2]
    score_scale = 1.0 / math.sqrt(key_cache.shape[3])
    positions = jnp.arange(cache_span, dtype=jnp.int32)
    live_mask = positions[None, :] < lengths[:, None]
    last_mask = positions[None, :] == lengths[:, None] - 1
    last_gate = jnp.sum(jnp.where(last_mask[:, None, :], gate_cache, 0.0), axis=-1)
    gate_now = last_gate + log_forget
    scores = (
        jnp.einsum("shd,shpd->shp", queries, key_cache, preferred_element_type=jnp.float32)
        * score_scale
    )
    scores = scores + gate_now[:, :, None] - gate_cache
    scores = jnp.where(live_mask[:, None, :], scores, -jnp.inf)
    own_score = (
        jnp.sum(queries.astype(jnp.float32) * keys_new.astype(jnp.float32), axis=-1) * score_scale
    )
    row_top = jnp.maximum(jnp.max(scores, axis=-1), own_score)
    raised = jnp.exp(scores - row_top[:, :, None])
    own_raised = jnp.exp(own_score - row_top)
    totals = jnp.sum(raised, axis=-1) + own_raised
    weights_low = (raised / totals[:, :, None]).astype(jnp.bfloat16)
    own_prob = (own_raised / totals).astype(jnp.bfloat16)
    attended = jnp.einsum(
        "shp,shpd->shd", weights_low, value_cache, preferred_element_type=jnp.float32
    )
    attended = attended + own_prob.astype(jnp.float32)[:, :, None] * values_new.astype(jnp.float32)
    return attended.astype(jnp.bfloat16)


def shards(
    tokens,
    attn_gain,
    query_weight,
    key_weight,
    value_weight,
    forget_weight,
    forget_bias,
    cache_keys,
    cache_values,
    cache_gates,
    lengths,
    output_weight,
    ffn_gain,
    dense_gate_proj,
    dense_up_proj,
    dense_down_proj,
    dense_mix,
    expert_ids,
    group_prob,
    pair_prob,
    expert_gate,
    expert_up,
    expert_down,
):
    seq_count, width = tokens.shape
    head_size = cache_keys.shape[3]
    chips = lax.axis_size(Z)
    quarters = lax.axis_size("zl")
    devices = lax.axis_size(EP)
    slab = width // chips
    core = lax.axis_index("c")

    own_rows = jnp.concatenate(
        (query_weight, key_weight, value_weight, dense_gate_proj, dense_up_proj), axis=1
    )
    their_rows = lax.ppermute(own_rows, "c", [(0, 1), (1, 0)])
    chip_rows = jnp.where(
        core == 0,
        jnp.concatenate((own_rows, their_rows), axis=0),
        jnp.concatenate((their_rows, own_rows), axis=0),
    )
    projection_width = 3 * head_size

    normed = rms_scale(tokens, attn_gain).astype(jnp.bfloat16)
    token_pieces = normed.reshape(seq_count, chips, slab).transpose(1, 0, 2)
    held = output_weight.shape[1]
    part = held // quarters
    out_parts = output_weight.T.reshape(quarters, part, head_size)
    down_parts = dense_down_proj.T.reshape(quarters, part, head_size)
    parts = jnp.tile(jnp.concatenate((out_parts, down_parts), axis=1), (chips // quarters, 1, 1))
    received = exchanged(jnp.concatenate((token_pieces, parts), axis=1), Z)
    token_columns = received[:, :seq_count].reshape(chips * seq_count, slab)
    out_quarter = received[:, seq_count : seq_count + part]
    down_quarter = received[:, seq_count + part :]

    def whole(quarter):
        gathered = lax.all_gather(quarter, ("zl", "c"), axis=0, tiled=False)
        gathered = gathered.reshape(quarters, 2, chips, part, head_size)
        return gathered.transpose(2, 1, 0, 3, 4).reshape(width, head_size)

    shares = product(token_columns, chip_rows[:, :projection_width]).astype(jnp.bfloat16)
    shares = exchanged(shares.reshape(chips, seq_count, projection_width), Z)
    output_columns = whole(out_quarter)
    projected = jnp.sum(shares.astype(jnp.float32), axis=0).astype(jnp.bfloat16)
    projected = projected.reshape(seq_count, 3, 1, head_size)
    log_forget = jax.nn.log_sigmoid(product(normed, forget_weight) + forget_bias)
    attended = attend(
        projected[:, 0],
        projected[:, 1],
        projected[:, 2],
        cache_keys,
        cache_values,
        cache_gates,
        lengths,
        log_forget,
    ).reshape(seq_count, head_size)
    head_terms = product_transposed(attended, output_columns).astype(jnp.bfloat16)
    down_columns = whole(down_quarter)
    residual = (tokens.astype(jnp.float32) + summed_over(head_terms, TP)).astype(jnp.bfloat16)
    ffn_in = rms_scale(residual, ffn_gain).astype(jnp.bfloat16)
    mix = jax.nn.sigmoid(product(ffn_in, dense_mix))

    picks = expert_ids.reshape(-1)
    capacity = 4 * seq_count // devices
    slot_total = devices * capacity
    pick_onehot = (picks[:, None] == jnp.arange(devices, dtype=jnp.int32)[None, :]).astype(jnp.int32)
    earlier = jnp.cumsum(pick_onehot, axis=0) - pick_onehot
    slot_rank = jnp.sum(earlier * pick_onehot, axis=1)
    destination = (picks * capacity + slot_rank).reshape(seq_count, 2)
    slot_grid = jnp.arange(slot_total, dtype=jnp.int32)
    select_first = (destination[:, 0:1] == slot_grid[None, :]).astype(jnp.bfloat16)
    select_second = (destination[:, 1:2] == slot_grid[None, :]).astype(jnp.bfloat16)
    outbound = jnp.einsum(
        "sk,sd->kd", select_first + select_second, ffn_in, preferred_element_type=jnp.float32
    )
    outbound = outbound.astype(jnp.bfloat16).reshape(devices, capacity, width)
    half = seq_count // 2
    across = half // capacity
    dense_pieces = ffn_in.reshape(2, across, capacity, chips, slab).transpose(3, 0, 2, 1, 4)
    dense_pieces = dense_pieces.reshape(devices, capacity, across * slab)
    arrived = exchanged(jnp.concatenate((outbound, dense_pieces), axis=2), EP)
    row_data = arrived[:, :, :width].reshape(slot_total, width)
    dense_rows = arrived[:, :, width:].reshape(devices, capacity, across, slab)
    dense_rows = dense_rows.transpose(0, 2, 1, 3).reshape(devices * half, slab)

    dense_shares = product(dense_rows, chip_rows[:, projection_width:]).astype(jnp.bfloat16)
    dense_width = dense_shares.shape[1]
    dense_shares = dense_shares.reshape(devices, capacity, across * dense_width)
    gate_part = product(row_data, expert_gate[0])
    up_part = product(row_data, expert_up[0])
    expert_hidden = (jax.nn.silu(gate_part) * up_part).astype(jnp.bfloat16)
    partial_out = product(expert_hidden, expert_down[0]).astype(jnp.bfloat16)
    back = exchanged(
        jnp.concatenate((partial_out.reshape(devices, capacity, width), dense_shares), axis=2), EP
    )
    returned = back[:, :, :width].reshape(slot_total, width)
    dense_parts = back[:, :, width:].reshape(chips, seq_count, dense_width)
    dense_parts = jnp.sum(dense_parts.astype(jnp.float32), axis=0)
    dense_hidden = jax.nn.silu(dense_parts[:, :head_size]) * dense_parts[:, head_size:]
    dense_terms = product_transposed(dense_hidden.astype(jnp.bfloat16), down_columns)
    routes = group_prob[:, None] * pair_prob / jnp.sum(pair_prob, axis=1, keepdims=True)
    side_total = (
        routes[:, 0:1] * product(select_first, returned)
        + routes[:, 1:2] * product(select_second, returned)
        + mix[:, None] * dense_terms
    )
    result = residual.astype(jnp.float32) + summed_over(side_total.astype(jnp.bfloat16), TP)
    return result.astype(jnp.bfloat16)


def solution(mesh):
    chips = mesh.shape["ep"] // 2
    finer = Mesh(mesh.devices.reshape(chips // 4, 4, 2, 4, 4), ("zh", "zl", "c", "y", "x"))
    in_specs = (
        P(EP, None),
        P(),
        P(EP, TP),
        P(EP, TP),
        P(EP, TP),
        P(None, TP),
        P(TP),
        P(EP, TP, None, None),
        P(EP, TP, None, None),
        P(EP, TP, None),
        P(EP),
        P(TP, EP),
        P(),
        P(EP, TP),
        P(EP, TP),
        P(TP, EP),
        P(),
        P(EP, None),
        P(EP),
        P(EP, None),
        P(EP, None, TP),
        P(EP, None, TP),
        P(EP, TP, None),
    )
    out_specs = P(EP, None)
    return jax.shard_map(
        shards, mesh=finer, in_specs=in_specs, out_specs=out_specs, check_vma=False
    )
```

time: 241 us -> 190 us (0.79)
  waiting for transfers between devices: 100 us -> 22.7 us
  blocking collectives: 59.3 us -> 106 us
  between operations: 14.4 us -> 1.16 us
  starting transfers between devices: 44.1 us -> 38.6 us
  matrix products: 10.6 us -> 6.52 us
  other arithmetic: 4.7 us -> 7.79 us
    all_gather x2 -> x0, waiting for transfers between devices: 80.8 us -> none  [sent_together(): filled = lax.all_gather(both, axis, axis=dim, tiled=True)]
    all_to_all x1 -> x2, blocking collectives: 18.7 us -> 56 us  [exchanged(): return lax.all_to_all(pieces, axes, split_axis=0, concat_axis=0, tiled=True)]
    all_gather x2, blocking collectives: 40.6 us -> 50.5 us  [whole(): gathered = lax.all_gather(quarter, ('zl', 'c'), axis=0, tiled=False)]
    all_to_all x4, starting transfers between devices: 44 us -> 35.7 us  [exchanged(): return lax.all_to_all(pieces, axes, split_axis=0, concat_axis=0, tiled=True)]
    dot_general x11, matrix products: 9.5 us -> 5.45 us  [the longest x8 4.6 us: product(): return jnp.dot(left, right, preferred_element_type=jnp.float32)]
    all_to_all x4, waiting for transfers between devices: 19.5 us -> 22.5 us  [exchanged(): return lax.all_to_all(pieces, axes, split_axis=0, concat_axis=0, tiled=True)]
    ppermute x0 -> x1, starting transfers between devices: none -> 2.86 us  [shards(): their_rows = lax.ppermute(own_rows, 'c', [(0, 1), (1, 0)])]
  transfers between devices with their start and end apart: 6 -> 5, of which waited for: 4 -> 3; matrix products, arithmetic and copies ran while one was open for 5% -> 2% of each run, Pallas kernels for 0% -> 0%
where the time goes in v1:
time: 190 us; the launch traced here: 189 us
  blocking collectives  106 us (56%)
  starting transfers between devices  38.6 us (20%)
  waiting for transfers between devices  22.7 us (12%)
  other arithmetic  7.79 us (4%)
  matrix products  6.52 us (3%)
  local copies, waits for them, and re-layouts  5.42 us (3%)
    all_to_all x2, blocking collectives, exchanged(): return lax.all_to_all(pieces, axes, split_axis=0, concat_axis=0, tiled=True)  56 us
    all_gather x2, blocking collectives, whole(): gathered = lax.all_gather(quarter, ('zl', 'c'), axis=0, tiled=False)  50.5 us
    all_to_all x4, starting transfers between devices, exchanged(): return lax.all_to_all(pieces, axes, split_axis=0, concat_axis=0, tiled=True)  35.7 us
    all_to_all x4, waiting for transfers between devices, exchanged(): return lax.all_to_all(pieces, axes, split_axis=0, concat_axis=0, tiled=True)  22.5 us
    dot_general x8, matrix products, product(): return jnp.dot(left, right, preferred_element_type=jnp.float32)  4.6 us
  transfers between devices with their start and end apart: 5, of which 3 were waited for; matrix products, arithmetic and copies ran while one was open for 2% of the time, Pallas kernels for 0%

profile of v1, /device:TPU:1, one launch (start us, length us, event | category | flops | bytes accessed | tf_op | source)
XLA Modules:
  0.0 188.7 jit_solution(11694490849298869871)
XLA Ops:
  0.0 1.1 fusion.19
  1.2 1.0 fusion.42
  2.2 0.7 pad_maximum_fusion.3
  2.9 0.7 pad_maximum_fusion.2
  3.6 15.7 %all-to-all-start = ((bf16[16,48,128]{2,1,0:T(8,128)(2,1)}), bf16[16,48,128]{2,1,0:T(8,128)(2,1)S(1)}, u32[]{:S(2)}, u32[]{:S(2)}) async-start(bf16[16,48,128]{2,1,0:T(8,128)(2,1)} %pad_maximum_fusion.2), calls=%async_computation | async-start | bytes 393216 | tf_op jit(solution)/shard_map/all_to_all | solution.py:16
  19.4 0.7 constant_dynamic-update-slice_fusion.4
  20.1 0.7 constant_dynamic-update-slice_fusion.3
  20.8 0.7 constant_dynamic-update-slice_fusion.2
  21.6 2.9 %collective-permute-start = (bf16[64,640]{1,0:T(8,128)(2,1)S(1)}, bf16[64,640]{1,0:T(8,128)(2,1)S(1)}, u32[]{:S(2)}, u32[]{:S(2)}) collective-permute-start(bf16[64,640]{1,0:T(8,128)(2,1)S(1)} %constant_dynamic-update-slice_fusion), channel_id=1, source_target_pairs={{0,16},{16,0},{1,17},{17,1},{2,18},{18,2},{3,19},{19,3},{4,20},{20... | collective-permute-start | bytes 245768 | tf_op jit(solution)/shard_map/ppermute | solution.py:109
  25.4 6.5 %all-to-all-done = bf16[16,48,128]{2,1,0:T(8,128)(2,1)S(1)} async-done(((bf16[16,48,128]{2,1,0:T(8,128)(2,1)}), bf16[16,48,128]{2,1,0:T(8,128)(2,1)S(1)}, u32[]{:S(2)}, u32[]{:S(2)}) %all-to-all-start) | async-done | bytes 196640 | tf_op jit(solution)/shard_map/all_to_all | solution.py:16
  31.9 0.9 convolution_convert_fusion.3
  32.7 8.9 %all-to-all-start.1 = ((bf16[16,16,384]{2,1,0:T(8,128)(2,1)}), bf16[16,16,384]{2,1,0:T(8,128)(2,1)S(1)}, u32[]{:S(2)}, u32[]{:S(2)}) async-start(bf16[16,16,384]{2,1,0:T(8,128)(2,1)} %bitcast.7), calls=%async_computation.1 | async-start | bytes 393216 | tf_op jit(solution)/shard_map/all_to_all | solution.py:16
  41.6 0.3 fusion.38
  42.2 21.2 %all-gather = bf16[128,16,128]{2,1,0:T(8,128)(2,1)S(1)} all-gather(bf16[16,16,128]{2,1,0:T(8,128)(2,1)S(1)} %get-tuple-element.10), channel_id=2, replica_groups=mesh['zh'=4,'zl'=4,'c'=2,'y'=4,'x'=4] {'zl','c'}, dimensions={0}, use_global_device_ids=true | all-gather | bytes 589824 | tf_op jit(solution)/shard_map/all_gather | solution.py:130
  63.8 0.6 fusion.5
  64.5 0.3 fusion.73
  64.8 0.3 fusion.71
  65.2 0.4 fusion.3
  65.6 0.3 convolution_convert_fusion.2
  65.9 1.1 broadcast_in_dim.13
  67.0 6.9 %all-to-all-start.2 = ((bf16[16,16,2048]{2,1,0:T(8,128)(2,1)}), bf16[16,16,2048]{2,1,0:T(8,128)(2,1)S(1)}, u32[]{:S(2)}, u32[]{:S(2)}) async-start(bf16[16,16,2048]{2,1,0:T(8,128)(2,1)} %broadcast_in_dim.13), calls=%async_computation.2 | async-start | bytes 2097152 | tf_op jit(solution)/shard_map/all_to_all | solution.py:16
  74.6 16.0 %all-to-all-done.2 = bf16[16,16,2048]{2,1,0:T(8,128)(2,1)S(1)} async-done(((bf16[16,16,2048]{2,1,0:T(8,128)(2,1)}), bf16[16,16,2048]{2,1,0:T(8,128)(2,1)S(1)}, u32[]{:S(2)}, u32[]{:S(2)}) %all-to-all-start.2) | async-done | bytes 1048608 | tf_op jit(solution)/shard_map/all_to_all | solution.py:16
  91.0 0.3 convolution_convert_fusion.1
  91.6 0.3 pad_maximum_fusion.1
  91.9 36.8 %all_to_all.30 = bf16[32,2,2560]{2,1,0:T(2,128)(2,1)S(1)} all-to-all(bf16[32,2,2560]{2,1,0:T(2,128)(2,1)S(1)} %pad_maximum_fusion.1), channel_id=1, replica_groups=mesh['zh'=4,'zl'=4,'c'=2,'y'=4,'x'=4] {'zh','zl','c'}, dimensions={0} | all-to-all | bytes 655360 | tf_op jit(solution)/shard_map/all_to_all | solution.py:16
  129.0 1.3 fusion.17
  130.2 1.5 convolution_convert_fusion
  132.2 1.1 pad_maximum_fusion
  133.3 4.3 %all-to-all-start.4 = ((bf16[32,2,3072]{2,1,0:T(2,128)(2,1)}), bf16[32,2,3072]{2,1,0:T(2,128)(2,1)S(1)}, u32[]{:S(2)}, u32[]{:S(2)}) async-start(bf16[32,2,3072]{2,1,0:T(2,128)(2,1)} %pad_maximum_fusion), calls=%async_computation.4 | async-start | bytes 786432 | tf_op jit(solution)/shard_map/all_to_all | solution.py:16
  137.7 29.2 %all-gather.1 = bf16[128,16,128]{2,1,0:T(8,128)(2,1)S(1)} all-gather(bf16[16,16,128]{2,1,0:T(8,128)(2,1)S(1)} %get-tuple-element.9), channel_id=3, replica_groups=mesh['zh'=4,'zl'=4,'c'=2,'y'=4,'x'=4] {'zl','c'}, dimensions={0}, use_global_device_ids=true | all-gather | bytes 589824 | tf_op jit(solution)/shard_map/all_gather | solution.py:130
  168.6 19.3 %all_to_all.31 = bf16[16,16,2048]{2,1,0:T(8,128)(2,1)S(1)} all-to-all(bf16[16,16,2048]{2,1,0:T(8,128)(2,1)S(1)} %broadcast_in_dim.14), channel_id=1, replica_groups=mesh['zh'=4,'zl'=4,'c'=2,'y'=4,'x'=4] {'y','x'}, dimensions={0} | all-to-all | bytes 2097152 | tf_op jit(solution)/shard_map/all_to_all | solution.py:16
  188.1 0.6 fusion.26
  (90 shorter events, 5.0 us)
Async XLA Ops:
  0.0 63.8 %copy-start = (bf16[16,1,384,128]{3,2,1,0:T(8,128)(2,1)S(1)}, bf16[16,1,384,128]{3,2,1,0:T(8,128)(2,1)}, u32[]{:S(2)}) copy-start(bf16[16,1,384,128]{3,2,1,0:T(8,128)(2,1)} %param.30) | copy-start | bytes 4718596
  0.0 21.5 %copy-start.5 = (bf16[64,128]{1,0:T(8,128)(2,1)S(1)}, bf16[64,128]{1,0:T(8,128)(2,1)}, u32[]{:S(2)}) copy-start(bf16[64,128]{1,0:T(8,128)(2,1)} %param.36) | copy-start | bytes 49156
  0.0 21.5 %copy-start.6 = (bf16[64,128]{1,0:T(8,128)(2,1)S(1)}, bf16[64,128]{1,0:T(8,128)(2,1)}, u32[]{:S(2)}) copy-start(bf16[64,128]{1,0:T(8,128)(2,1)} %param.37) | copy-start | bytes 49156
  0.0 41.6 %copy-start.11 = (s32[16]{0:T(128)S(1)}, s32[16]{0:T(128)}, u32[]{:S(2)}) copy-start(s32[16]{0:T(128)} %param.33) | copy-start | bytes 196
  0.0 41.6 %copy-start.3 = (f32[16,1,384]{2,1,0:T(1,128)S(1)}, f32[16,1,384]{2,1,0:T(1,128)}, u32[]{:S(2)}) copy-start(f32[16,1,384]{2,1,0:T(1,128)} %param.32) | copy-start | bytes 73732
  1.1 40.8 %copy-start.1 = (bf16[16,2048]{1,0:T(8,128)(2,1)S(1)}, bf16[16,2048]{1,0:T(8,128)(2,1)}, u32[]{:S(2)}) copy-start(bf16[16,2048]{1,0:T(8,128)(2,1)} %param.23) | copy-start | bytes 196612
  1.1 40.8 %copy-start.7 = (f32[2048]{0:T(1024)S(1)}, f32[2048]{0:T(1024)}, u32[]{:S(2)}) copy-start(f32[2048]{0:T(1024)} %param.24) | copy-start | bytes 24580
  1.1 40.8 %copy-start.14 = (bf16[2048,1]{0,1:T(2,128)(2,1)S(1)}, bf16[2048,1]{0,1:T(2,128)(2,1)}, u32[]{:S(2)}) copy-start(bf16[2048,1]{0,1:T(2,128)(2,1)} %param.28) | copy-start | bytes 12292
  3.6 28.2 %all-to-all-start = ((bf16[16,48,128]{2,1,0:T(8,128)(2,1)}), bf16[16,48,128]{2,1,0:T(8,128)(2,1)S(1)}, u32[]{:S(2)}, u32[]{:S(2)}) async-start(bf16[16,48,128]{2,1,0:T(8,128)(2,1)} %pad_maximum_fusion.2), calls=%async_computation | async-start | bytes 393216 | tf_op jit(solution)/shard_map/all_to_all | solution.py:16
  21.6 3.8 %collective-permute-start = (bf16[64,640]{1,0:T(8,128)(2,1)S(1)}, bf16[64,640]{1,0:T(8,128)(2,1)S(1)}, u32[]{:S(2)}, u32[]{:S(2)}) collective-permute-start(bf16[64,640]{1,0:T(8,128)(2,1)S(1)} %constant_dynamic-update-slice_fusion), channel_id=1, source_target_pairs={{0,16},{16,0},{1,17},{17,1},{2,18},{18,2},{3,19},{19,3},{4,20},{20... | collective-permute-start | bytes 245768 | tf_op jit(solution)/shard_map/ppermute | solution.py:109
  32.7 30.7 %all-to-all-start.1 = ((bf16[16,16,384]{2,1,0:T(8,128)(2,1)}), bf16[16,16,384]{2,1,0:T(8,128)(2,1)S(1)}, u32[]{:S(2)}, u32[]{:S(2)}) async-start(bf16[16,16,384]{2,1,0:T(8,128)(2,1)} %bitcast.7), calls=%async_computation.1 | async-start | bytes 393216 | tf_op jit(solution)/shard_map/all_to_all | solution.py:16
  63.5 1.6 copy-start.13
  65.9 8.0 %copy-start.9 = (s32[16,2]{0,1:T(2,128)S(1)}, s32[16,2]{0,1:T(2,128)}, u32[]{:S(2)}) copy-start(s32[16,2]{0,1:T(2,128)} %param.40) | copy-start | bytes 388
  67.0 23.9 %copy-start.4 = (f32[2048]{0:T(1024)S(1)}, f32[2048]{0:T(1024)}, u32[]{:S(2)}) copy-start(f32[2048]{0:T(1024)} %param.35) | copy-start | bytes 24580
  67.0 23.6 %all-to-all-start.2 = ((bf16[16,16,2048]{2,1,0:T(8,128)(2,1)}), bf16[16,16,2048]{2,1,0:T(8,128)(2,1)S(1)}, u32[]{:S(2)}, u32[]{:S(2)}) async-start(bf16[16,16,2048]{2,1,0:T(8,128)(2,1)} %broadcast_in_dim.13), calls=%async_computation.2 | async-start | bytes 2097152 | tf_op jit(solution)/shard_map/all_to_all | solution.py:16
  91.6 38.6 %copy-start.2 = (bf16[1,128,2048]{2,1,0:T(8,128)(2,1)S(1)}, bf16[1,128,2048]{2,1,0:T(8,128)(2,1)}, u32[]{:S(2)}) copy-start(bf16[1,128,2048]{2,1,0:T(8,128)(2,1)} %param.45) | copy-start | bytes 1572868
  131.7 5.9 %copy-start.8 = (bf16[2048]{0:T(1024)(128)(2,1)S(1)}, bf16[2048]{0:T(1024)(128)(2,1)}, u32[]{:S(2)}) copy-start(bf16[2048]{0:T(1024)(128)(2,1)} %param.39) | copy-start | bytes 12292
  131.7 5.9 %copy-start.10 = (f32[16,2]{0,1:T(2,128)S(1)}, f32[16,2]{0,1:T(2,128)}, u32[]{:S(2)}) copy-start(f32[16,2]{0,1:T(2,128)} %param.42) | copy-start | bytes 388
  131.7 5.9 %copy-start.12 = (f32[16]{0:T(128)S(1)}, f32[16]{0:T(128)}, u32[]{:S(2)}) copy-start(f32[16]{0:T(128)} %param.41) | copy-start | bytes 196
  133.3 33.9 %all-to-all-start.4 = ((bf16[32,2,3072]{2,1,0:T(2,128)(2,1)}), bf16[32,2,3072]{2,1,0:T(2,128)(2,1)S(1)}, u32[]{:S(2)}, u32[]{:S(2)}) async-start(bf16[32,2,3072]{2,1,0:T(2,128)(2,1)} %pad_maximum_fusion), calls=%async_computation.4 | async-start | bytes 786432 | tf_op jit(solution)/shard_map/all_to_all | solution.py:16
